TPU v7x, 32 devices: a whole 2x2x4 slice. The times are simulated.
32 devices in a mesh: ep: 8 (over z, y), tp: 4 (over x, core).
Axes of the slice: x: 2, y: 2, z: 4, core: 2. Of those that a mesh axis runs over, the one named last changes fastest.
Arguments:
- tokens: bfloat16 [256, 2048], P('ep', 'tp'), may hold values from -33 to 33
- previous: bfloat16 [256, 2048], P('ep', 'tp'), may hold values from -6 to 6
- first_norm_gain: float32 [2048], replicated, may hold values from 0.1 to 1.9
- token_shift_share: float32 [5, 2048], replicated, may hold values from 0 to 1
- receptance_weight: bfloat16 [2048, 1024], P(None, 'tp'), may hold values from -0.125 to 0.125
- key_weight: bfloat16 [2048, 1024], P(None, 'tp'), may hold values from -0.125 to 0.125
- value_weight: bfloat16 [2048, 1024], P(None, 'tp'), may hold values from -0.125 to 0.125
- decay_down_map: bfloat16 [2048, 128], replicated, may hold values from -0.125 to 0.125
- decay_up_map: bfloat16 [128, 1024], replicated, may hold values from -0.5 to 0.5
- decay_offset: float32 [1024], P('tp'), may hold values from -4 to 1
- strength_down_map: bfloat16 [2048, 128], replicated, may hold values from -0.125 to 0.125
- strength_up_map: bfloat16 [128, 1024], replicated, may hold values from -0.5 to 0.5
- removal_key_scale: float32 [1024], P('tp'), may hold values from 0.3 to 3
- key_damping: float32 [1024], P('tp'), may hold values from 0.1 to 1.9
- self_term_weight: float32 [16, 64], P('tp'), may hold values from -0.6 to 0.6
- head_norm_gain: float32 [1024], P('tp'), may hold values from 0.1 to 1.9
- output_weight: bfloat16 [1024, 2048], P('tp'), may hold values from -0.1875 to 0.1875
- state: float32 [256, 16, 64, 64], P('ep', 'tp'), may hold values from -6 to 6
- second_norm_gain: float32 [2048], replicated, may hold values from 0.1 to 1.9
- routes: int32 [256, 4], P('ep'), may hold values from 0 to 7, all different within a row; in each aligned block of 32 rows (0 to 31, 32 to 63, ...) at most 24 rows name the same one
- chosen_expert_weight: float32 [256, 4], P('ep'), may hold values from 0.1 to 1
- expert_gate_weight: bfloat16 [8, 2048, 1024], P('ep', None, 'tp'), may hold values from -0.5 to 0.5
- expert_up_weight: bfloat16 [8, 2048, 1024], P('ep', None, 'tp'), may hold values from -0.5 to 0.5
- expert_down_weight: bfloat16 [8, 1024, 2048], P('ep', 'tp'), may hold values from -0.046875 to 0.046875
Outputs:
- layer_out: bfloat16 [256, 2048], P('ep', 'tp')
- new_state: float32 [256, 16, 64, 64], P('ep', 'tp')
Inputs may be any that keep to these rules, and one draw needn't show every extreme that they name: `routes`: each row names 4 different experts. Among the rows of one index of ep no expert is named by more than 24 rows, and in every draw some expert is named by exactly 24 rows of some index of ep.
All inputs are finite; a program needn't handle non-finite values.
Results may differ from a plain program's by a relative error of at most 0.015.
Values may be sent and summed in bfloat16 or wider, within the bound.
A program may use at most 64 MiB of HBM per device.

v0:
```python
import jax
import jax.numpy as jnp
from jax import lax
from jax.sharding import PartitionSpec as P

NORM_EPS = 1e-06
GROUP_EPS = 0.00064
KEY_EPS = 1e-06
GATE_LIMIT = 7.0
GATE_SLOPE = 1.702


def row_rescale(values, gain):
    return values * lax.rsqrt(jnp.mean(values * values, axis=-1, keepdims=True) + NORM_EPS) * gain


def head_combiner(
    present_rows,
    prior_rows,
    first_norm_gain,
    token_shift_share,
    receptance_weight,
    key_weight,
    value_weight,
    decay_down_map,
    decay_up_map,
    decay_offset,
    strength_down_map,
    strength_up_map,
    removal_key_scale,
    key_damping,
    self_term_weight,
    head_norm_gain,
    state,
):
    sequence_count = present_rows.shape[0]
    head_number = state.shape[1]
    head_extent = state.shape[2]
    normed = row_rescale(present_rows.astype(jnp.float32), first_norm_gain)
    before = prior_rows.astype(jnp.float32)

    def shifted(role):
        return (normed + (before - normed) * token_shift_share[role]).astype(jnp.bfloat16)

    def project(inputs, weight):
        return jnp.dot(inputs, weight, preferred_element_type=jnp.float32)

    def by_heads(values):
        return values.reshape(sequence_count, head_number, head_extent)

    receptance_rows = by_heads(project(shifted(0), receptance_weight))
    key_rows = by_heads(project(shifted(1), key_weight))
    value_matrix = by_heads(project(shifted(2), value_weight))
    decay_low = jnp.tanh(project(shifted(3), decay_down_map)).astype(jnp.bfloat16)
    decay_pre = decay_offset + project(decay_low, decay_up_map)
    decay = by_heads(jnp.exp(-jnp.exp(-jax.nn.softplus(-decay_pre) - 0.5)))
    alpha_low = project(shifted(4), strength_down_map).astype(jnp.bfloat16)
    alpha = by_heads(jax.nn.sigmoid(project(alpha_low, strength_up_map)))
    removal = key_rows * removal_key_scale.reshape(head_number, head_extent)
    removal = removal * lax.rsqrt(jnp.sum(removal * removal, axis=-1, keepdims=True) + KEY_EPS)
    blended_rows = key_rows * (1.0 + (alpha - 1.0) * key_damping.reshape(head_number, head_extent))
    highest = lax.Precision.HIGHEST
    along = jnp.einsum("shij,shj->shi", state, removal, precision=highest)
    new_state = (
        state * decay[:, :, None, :]
        - along[..., None] * (removal * alpha)[:, :, None, :]
        + value_matrix[..., None] * blended_rows[:, :, None, :]
    )
    readout = jnp.einsum("shij,shj->shi", new_state, receptance_rows, precision=highest)
    centered = readout - jnp.mean(readout, axis=-1, keepdims=True)
    variance = jnp.mean(centered * centered, axis=-1, keepdims=True)
    heads_normalised = (
        centered
        * lax.rsqrt(variance + GROUP_EPS)
        * head_norm_gain.reshape(head_number, head_extent)
    )
    self_term = (
        jnp.sum(receptance_rows * blended_rows * self_term_weight, axis=-1, keepdims=True)
        * value_matrix
    )
    mixed_inputs = (
        (heads_normalised + self_term)
        .reshape(sequence_count, head_number * head_extent)
        .astype(jnp.bfloat16)
    )
    return (mixed_inputs, new_state)


def shards(
    tokens,
    previous,
    first_norm_gain,
    token_shift_share,
    receptance_weight,
    key_weight,
    value_weight,
    decay_down_map,
    decay_up_map,
    decay_offset,
    strength_down_map,
    strength_up_map,
    removal_key_scale,
    key_damping,
    self_term_weight,
    head_norm_gain,
    output_weight,
    state,
    second_norm_gain,
    routes,
    chosen_expert_weight,
    expert_gate_weight,
    expert_up_weight,
    expert_down_weight,
):
    present_rows, prior_rows = (
        lax.all_gather(tokens, "tp", axis=1, tiled=True),
        lax.all_gather(previous, "tp", axis=1, tiled=True),
    )
    head_columns = receptance_weight.shape[1]
    head_start = lax.axis_index("tp") * head_columns
    decay_own = lax.dynamic_slice_in_dim(decay_up_map, head_start, head_columns, 1)
    alpha_own = lax.dynamic_slice_in_dim(strength_up_map, head_start, head_columns, 1)
    mixed_inputs, new_state = head_combiner(
        present_rows,
        prior_rows,
        first_norm_gain,
        token_shift_share,
        receptance_weight,
        key_weight,
        value_weight,
        decay_down_map,
        decay_own,
        decay_offset,
        strength_down_map,
        alpha_own,
        removal_key_scale,
        key_damping,
        self_term_weight,
        head_norm_gain,
        state,
    )
    head_terms = jnp.dot(mixed_inputs, output_weight, preferred_element_type=jnp.float32)
    own_columns = tokens.shape[1]
    column_start = lax.axis_index("tp") * own_columns
    residual = present_rows.astype(jnp.float32) + lax.psum(
        head_terms.astype(jnp.bfloat16), "tp"
    ).astype(jnp.float32)
    expert_rows = row_rescale(residual, second_norm_gain).astype(jnp.bfloat16)
    residual_own = lax.dynamic_slice_in_dim(residual, column_start, own_columns, 1)
    normed_own = lax.dynamic_slice_in_dim(expert_rows, column_start, own_columns, 1)
    sequences, choices_per = routes.shape
    experts = expert_gate_weight.shape[0] * lax.axis_size("ep")
    capacity = max(2, 3 * sequences * choices_per // (2 * experts))
    flattened = routes.reshape(-1)
    onehot = (flattened[:, None] == jnp.arange(experts, dtype=jnp.int32)[None, :]).astype(jnp.int32)
    ranking = jnp.sum((jnp.cumsum(onehot, axis=0) - onehot) * onehot, axis=1)
    slot_index = flattened * capacity + ranking
    placing = jnp.arange(experts * capacity, dtype=jnp.int32)[:, None] == slot_index[None, :]
    dispatch = jnp.sum(
        placing.reshape(experts * capacity, sequences, choices_per).astype(jnp.int32), axis=2
    ).astype(jnp.bfloat16)
    outgoing = jnp.dot(dispatch, normed_own, preferred_element_type=jnp.float32).astype(
        jnp.bfloat16
    )
    outgoing = outgoing.reshape(experts, capacity, -1)
    arrived = lax.all_gather(
        lax.all_to_all(outgoing, "ep", split_axis=0, concat_axis=0, tiled=True),
        "tp",
        axis=2,
        tiled=True,
    )
    sources, slot_count, feature_count = arrived.shape
    expert_input = arrived.reshape(sources * slot_count, feature_count)
    gate_pre = jnp.minimum(
        jnp.dot(expert_input, expert_gate_weight[0], preferred_element_type=jnp.float32), GATE_LIMIT
    )
    up_pre = jnp.clip(
        jnp.dot(expert_input, expert_up_weight[0], preferred_element_type=jnp.float32),
        -GATE_LIMIT,
        GATE_LIMIT,
    )
    activation = ((up_pre + 1.0) * gate_pre * jax.nn.sigmoid(GATE_SLOPE * gate_pre)).astype(
        jnp.bfloat16
    )
    down_terms = jnp.dot(activation, expert_down_weight[0], preferred_element_type=jnp.float32)
    down_terms = down_terms.reshape(sources, slot_count, -1)
    shares = lax.psum_scatter(
        down_terms.astype(jnp.bfloat16), "tp", scatter_dimension=2, tiled=True
    )
    returned = lax.all_to_all(shares, "ep", split_axis=0, concat_axis=0, tiled=True)
    returned_rows = returned.reshape(experts * capacity, -1)
    picked = jnp.take(returned_rows, slot_index, axis=0).astype(jnp.float32)
    weighted = jnp.sum(
        picked.reshape(sequences, choices_per, -1) * chosen_expert_weight[:, :, None], axis=1
    )
    layer_out = (residual_own + weighted).astype(jnp.bfloat16)
    return (layer_out, new_state)


def solution(mesh):
    in_specs = (
        P("ep", "tp"),
        P("ep", "tp"),
        P(),
        P(),
        P(None, "tp"),
        P(None, "tp"),
        P(None, "tp"),
        P(),
        P(),
        P("tp"),
        P(),
        P(),
        P("tp"),
        P("tp"),
        P("tp", None),
        P("tp"),
        P("tp", None),
        P("ep", "tp", None, None),
        P(),
        P("ep", None),
        P("ep", None),
        P("ep", None, "tp"),
        P("ep", None, "tp"),
        P("ep", "tp", None),
    )
    out_specs = (P("ep", "tp"), P("ep", "tp", None, None))
    return jax.shard_map(shards, mesh=mesh, in_specs=in_specs, out_specs=out_specs, check_vma=False)
```

profile of v0, /device:TPU:0, one launch (start us, length us, event | category | flops | bytes accessed | tf_op | source)
XLA Modules:
  0.0 153.4 jit_solution(18078987325772897809)
XLA Ops:
  7.3 6.9 %all_gather.9 = bf16[32,2048]{1,0:T(8,128)(2,1)S(1)} all-gather(bf16[32,512]{1,0:T(8,128)(2,1)} %param.24), channel_id=1, replica_groups=mesh['ep'=8,'tp'=4] {'tp'}, dimensions={1}, use_global_device_ids=true | all-gather | bytes 163840 | tf_op jit(solution)/shard_map/all_gather | solution.py:116
  14.1 0.1 fusion.16
  14.3 5.8 %all_gather.10 = bf16[32,2048]{1,0:T(8,128)(2,1)S(1)} all-gather(bf16[32,512]{1,0:T(8,128)(2,1)} %param.25), channel_id=1, replica_groups=mesh['ep'=8,'tp'=4] {'tp'}, dimensions={1}, use_global_device_ids=true | all-gather | bytes 163840 | tf_op jit(solution)/shard_map/all_gather | solution.py:117
  20.1 1.1 fusion.83
  21.2 1.6 %fusion.29 = f32[32,256]{1,0:T(8,128)S(1)} fusion(bf16[2048,256]{1,0:T(8,128)(2,1)} %param.28, bf16[32,2048]{1,0:T(8,128)(2,1)S(1)} %all_gather.9, bf16[32,2048]{1,0:T(8,128)(2,1)S(1)} %all_gather.10, f32[2048]{0:T(1024)S(1)} %bitcast.60, f32[2048]{0:T(1024)} %param.26, f32[32]{0:T(128)S(1)} %add_rsqrt_fusion.3), kind=kOutput, calls=%fused_computation.45 | convolution fusion | flops 34078720 | bytes 1360000 | tf_op jit(solution)/shard_map/dot_general | solution.py:46
  22.7 0.1 reshape.176
  22.8 0.7 reshape.161
  23.5 1.4 fusion.10
  25.0 0.1 reshape.160
  25.1 1.6 %fusion.35 = f32[32,256]{1,0:T(8,128)S(1)} fusion(bf16[2048,256]{1,0:T(8,128)(2,1)} %param.29, bf16[32,2048]{1,0:T(8,128)(2,1)S(1)} %all_gather.9, bf16[32,2048]{1,0:T(8,128)(2,1)S(1)} %all_gather.10, f32[2048]{0:T(1024)S(1)} %bitcast.59, f32[2048]{0:T(1024)} %param.26, f32[32]{0:T(128)S(1)} %add_rsqrt_fusion.3), kind=kOutput, calls=%fused_computation.47 | convolution fusion | flops 34078720 | bytes 1360000 | tf_op jit(solution)/shard_map/dot_general | solution.py:46
  26.6 0.1 reshape.159
  26.8 0.1 multiply_reduce_fusion.3
  27.1 1.3 fusion.67
  28.3 0.1 mul.284
  28.5 0.3 fusion.31
  28.8 0.1 mul.306
  28.9 0.1 fusion.82
  29.0 8.5 %fusion.84 = f32[32,4,1,64]{3,2,1,0:T(1,128)S(1)} fusion(f32[32,4,64,1]{2,3,1,0:T(1,128)S(1)} %bitcast.56, f32[32,4,64,64]{3,2,1,0:T(8,128)} %param.41), kind=kOutput, calls=%fused_computation.105 | convolution fusion | flops 6291456 | bytes 2162688 | tf_op jit(solution)/shard_map/shij,shj->shi/dot_general | solution.py:63
  37.5 2.8 %multiply_add_fusion = f32[32,4,64,64]{3,2,1,0:T(8,128)S(1)} fusion(f32[32,4,64,64]{3,2,1,0:T(8,128)S(1)} %copy-done.1, f32[32,4,64]{2,1,0:T(4,128)S(1)} %get-tuple-element.8, f32[32,4,64]{2,1,0:T(4,128)S(1)} %mul.306, f32[32,4,64]{2,1,0:T(4,128)S(1)} %get-tuple-element.4, f32[32,4,64]{2,1,0:T(4,128)S(1)} %bitcast.54, f32[32,4,64]{2,1,0:T(4,128)S(1)} %mul.284), kind=kLoop, calls=%fused_computation.2 | loop fusion | flops 2621440 | bytes 4358144 | tf_op jit(solution)/shard_map/add | solution.py:65
  40.4 2.0 %copy-done.2 = f32[32,4,64,64]{3,2,1,0:T(8,128)} copy-done((f32[32,4,64,64]{3,2,1,0:T(8,128)}, f32[32,4,64,64]{3,2,1,0:T(8,128)S(1)}, u32[]{:S(2)}) %copy-start.2) | copy-done | bytes 2097176
  42.3 6.6 %fusion.85 = f32[32,4,1,64]{3,2,1,0:T(1,128)S(1)} fusion(f32[32,4,64,64]{3,2,1,0:T(8,128)S(1)} %multiply_add_fusion, f32[32,4,64,1]{2,3,1,0:T(1,128)S(1)} %bitcast.55), kind=kOutput, calls=%fused_computation.106 | convolution fusion | flops 6291456 | bytes 2162688 | tf_op jit(solution)/shard_map/shij,shj->shi/dot_general | solution.py:69
  48.9 0.1 reduce_sum.87
  49.1 0.2 multiply_reduce_fusion.2
  49.2 0.6 add_rsqrt_fusion
  49.9 1.4 fusion.7
  51.3 0.1 convert_element_type.78
  51.4 0.9 convolution_convert_fusion.1
  52.5 0.1 reshape.162
  52.7 0.2 reduce_window_sum.11
  52.9 0.2 select_reduce_fusion
  53.1 0.1 reduce_sum.91
  53.3 0.8 dynamic-slice
  54.2 31.7 %all-reduce.2.cloned.1.call-done = bf16[32,2048]{1,0:T(8,128)(2,1)} async-done(((bf16[32,2048]{1,0:T(8,128)(2,1)}), bf16[32,2048]{1,0:T(8,128)(2,1)}) %all-reduce.2.cloned.1.call-update) | async-done | bytes 131088 | tf_op jit(solution)/shard_map/psum | solution.py:145
  85.8 1.1 multiply_reduce_fusion.1
  87.0 0.3 convolution_convert_fusion.2
  87.3 13.1 %all_to_all.10 = bf16[8,24,512]{2,1,0:T(8,128)(2,1)S(1)} all-to-all(bf16[8,24,512]{2,1,0:T(8,128)(2,1)S(1)} %bitcast.50), channel_id=1, replica_groups=mesh['ep'=8,'tp'=4] {'ep'}, dimensions={0} | all-to-all | bytes 393216 | tf_op jit(solution)/shard_map/all_to_all | solution.py:167
  100.3 7.6 %all_gather.11 = bf16[8,24,2048]{2,1,0:T(8,128)(2,1)S(1)} all-gather(bf16[8,24,512]{2,1,0:T(8,128)(2,1)S(1)} %all_to_all.10), channel_id=1, replica_groups=mesh['ep'=8,'tp'=4] {'tp'}, dimensions={2}, use_global_device_ids=true | all-gather | bytes 983040 | tf_op jit(solution)/shard_map/all_gather | solution.py:166
  107.9 0.4 convolution_minimum_fusion
  108.3 0.4 fusion.4
  108.7 1.3 convolution_convert_fusion
  110.0 21.4 %reduce-scatter.2.cloned.1.call-done = bf16[8,24,512]{2,1,0:T(8,128)(2,1)} async-done(((bf16[8,24,2048]{2,1,0:T(8,128)(2,1)}), bf16[8,24,512]{2,1,0:T(8,128)(2,1)}) %reduce-scatter.2.cloned.1.call-update) | async-done | bytes 196624 | tf_op jit(solution)/shard_map/reduce_scatter | solution.py:187
  131.5 5.5 %all-to-all-start.1 = ((bf16[8,24,512]{2,1,0:T(8,128)(2,1)}), bf16[8,24,512]{2,1,0:T(8,128)(2,1)S(1)}, u32[]{:S(2)}, u32[]{:S(2)}) async-start(bf16[8,24,512]{2,1,0:T(8,128)(2,1)} %reduce-scatter.2.cloned.1.call-done), calls=%async_computation.2 | async-start | bytes 393216 | tf_op jit(solution)/shard_map/all_to_all | solution.py:190
  137.1 0.1 mul.341
  137.2 0.1 copy.38
  137.4 7.4 %all-to-all-done.1 = bf16[8,24,512]{2,1,0:T(8,128)(2,1)S(1)} async-done(((bf16[8,24,512]{2,1,0:T(8,128)(2,1)}), bf16[8,24,512]{2,1,0:T(8,128)(2,1)S(1)}, u32[]{:S(2)}, u32[]{:S(2)}) %all-to-all-start.1) | async-done | bytes 196640 | tf_op jit(solution)/shard_map/all_to_all | solution.py:190
  144.8 0.8 gather_fusion
  145.7 0.3 multiply_reduce_fusion
  145.9 0.6 add_convert_fusion
  (53 shorter events, 1.0 us)
Async XLA Ops:
  7.2 101.6 %copy-start = (bf16[1,256,2048]{2,1,0:T(8,128)(2,1)S(1)}, bf16[1,256,2048]{2,1,0:T(8,128)(2,1)}, u32[]{:S(2)}) copy-start(bf16[1,256,2048]{2,1,0:T(8,128)(2,1)} %param.47) | copy-start | bytes 3145732
  7.2 19.9 %copy-start.6 = (f32[2048]{0:T(1024)S(1)}, f32[2048]{0:T(1024)}, u32[]{:S(2)}) copy-start(f32[2048]{0:T(1024)} %param.26) | copy-start | bytes 24580
  7.2 19.6 %copy-start.9 = (f32[256]{0:T(256)S(1)}, f32[256]{0:T(256)}, u32[]{:S(2)}) copy-start(f32[256]{0:T(256)} %param.36) | copy-start | bytes 3076
  7.2 19.8 %copy-start.10 = (f32[256]{0:T(256)S(1)}, f32[256]{0:T(256)}, u32[]{:S(2)}) copy-start(f32[256]{0:T(256)} %param.37) | copy-start | bytes 3076
  7.2 19.9 %copy-start.13 = (bf16[2048,128]{1,0:T(8,128)(2,1)S(1)}, bf16[2048,128]{1,0:T(8,128)(2,1)}, u32[]{:S(2)}) copy-start(bf16[2048,128]{1,0:T(8,128)(2,1)} %param.31) | copy-start | bytes 1572868
  7.2 19.8 %copy-start.15 = (f32[256]{0:T(256)S(1)}, f32[256]{0:T(256)}, u32[]{:S(2)}) copy-start(f32[256]{0:T(256)} %param.33) | copy-start | bytes 3076
  7.2 21.2 %copy-start.3 = (bf16[2048,256]{1,0:T(8,128)(2,1)S(1)}, bf16[2048,256]{1,0:T(8,128)(2,1)}, u32[]{:S(2)}) copy-start(bf16[2048,256]{1,0:T(8,128)(2,1)} %param.30) | copy-start | bytes 3145732
  7.2 78.6 %all-reduce.2.cloned.1.call-start = ((), (), s32[]{:S(2)}) async-start(), calls=%async_computation.3 | async-start | bytes 262144 | tf_op jit(solution)/shard_map/psum | solution.py:145
  28.9 8.7 %copy-start.1 = (f32[32,4,64,64]{3,2,1,0:T(8,128)S(1)}, f32[32,4,64,64]{3,2,1,0:T(8,128)}, u32[]{:S(2)}) copy-start(f32[32,4,64,64]{3,2,1,0:T(8,128)} %param.41) | copy-start | bytes 6291460
  40.3 2.0 %copy-start.2 = (f32[32,4,64,64]{3,2,1,0:T(8,128)}, f32[32,4,64,64]{3,2,1,0:T(8,128)S(1)}, u32[]{:S(2)}) copy-start(f32[32,4,64,64]{3,2,1,0:T(8,128)S(1)} %multiply_add_fusion) | copy-start | bytes 6291460
  40.3 9.5 %copy-start.11 = (f32[256]{0:T(256)S(1)}, f32[256]{0:T(256)}, u32[]{:S(2)}) copy-start(f32[256]{0:T(256)} %param.39) | copy-start | bytes 3076
  40.3 9.6 %copy-start.14 = (f32[4,64]{1,0:T(4,128)S(1)}, f32[4,64]{1,0:T(4,128)}, u32[]{:S(2)}) copy-start(f32[4,64]{1,0:T(4,128)} %param.38) | copy-start | bytes 3076
  40.4 11.1 %copy-start.4 = (bf16[256,2048]{1,0:T(8,128)(2,1)S(1)}, bf16[256,2048]{1,0:T(8,128)(2,1)}, u32[]{:S(2)}) copy-start(bf16[256,2048]{1,0:T(8,128)(2,1)} %param.40) | copy-start | bytes 3145732
  40.4 12.1 %copy-start.7 = (s32[32,4]{0,1:T(4,128)S(1)}, s32[32,4]{0,1:T(4,128)}, u32[]{:S(2)}) copy-start(s32[32,4]{0,1:T(4,128)} %param.43) | copy-start | bytes 1540
  42.3 65.6 %copy-start.5 = (bf16[1,2048,256]{2,1,0:T(8,128)(2,1)S(1)}, bf16[1,2048,256]{2,1,0:T(8,128)(2,1)}, u32[]{:S(2)}) copy-start(bf16[1,2048,256]{2,1,0:T(8,128)(2,1)} %param.45) | copy-start | bytes 3145732
  52.4 79.1 %reduce-scatter.2.cloned.1.call-start = ((), (), s32[]{:S(2)}) async-start(), calls=%async_computation.4 | async-start | bytes 983040 | tf_op jit(solution)/shard_map/reduce_scatter | solution.py:187
  85.8 22.5 %copy-start.12 = (bf16[1,2048,256]{2,1,0:T(8,128)(2,1)S(1)}, bf16[1,2048,256]{2,1,0:T(8,128)(2,1)}, u32[]{:S(2)}) copy-start(bf16[1,2048,256]{2,1,0:T(8,128)(2,1)} %param.46) | copy-start | bytes 3145732
  107.9 29.4 %copy-start.8 = (f32[32,4]{0,1:T(4,128)S(1)}, f32[32,4]{0,1:T(4,128)}, u32[]{:S(2)}) copy-start(f32[32,4]{0,1:T(4,128)} %param.44) | copy-start | bytes 1540
  131.5 13.3 %all-to-all-start.1 = ((bf16[8,24,512]{2,1,0:T(8,128)(2,1)}), bf16[8,24,512]{2,1,0:T(8,128)(2,1)S(1)}, u32[]{:S(2)}, u32[]{:S(2)}) async-start(bf16[8,24,512]{2,1,0:T(8,128)(2,1)} %reduce-scatter.2.cloned.1.call-done), calls=%async_computation.2 | async-start | bytes 393216 | tf_op jit(solution)/shard_map/all_to_all | solution.py:190
Sparse Core Ops, SparseCore 0:
  52.5 33.2 all-reduce.1
  110.1 21.2 reduce-scatter.1
where the time goes:
time: 154 us; the launch traced here: 153 us
  waiting for transfers between devices  60.5 us (39%)
  blocking collectives  33.3 us (22%)
  matrix products  24.5 us (16%)
  between operations  14.4 us (9%)
  other arithmetic  7.99 us (5%)
  local copies, waits for them, and re-layouts  7.04 us (5%)
  starting transfers between devices  5.62 us (4%)
    psum x1, waiting for transfers between devices, shards(): lax.psum(head_terms.astype(jnp.bfloat16), 'tp').astype(jnp.float32)  31.7 us
    reduce_scatter x1, waiting for transfers between devices, shards(): lax.psum_scatter(down_terms.astype(jnp.bfloat16), 'tp', scatter_dimension...  21.4 us
    all_to_all x1, blocking collectives, shards(): lax.all_to_all(outgoing, 'ep', split_axis=0, concat_axis=0, tiled=True)  13.1 us
    dot_general x1, matrix products, head_combiner(): along = jnp.einsum('shij,shj->shi', state, removal, precision=highest)  8.53 us
    all_gather x1, blocking collectives, shards(): lax.all_gather(lax.all_to_all(outgoing, 'ep', split_axis=0, concat_axis=0...  7.59 us
    all_to_all x1, waiting for transfers between devices, shards(): lax.all_to_all(shares, 'ep', split_axis=0, concat_axis=0, tiled=True)  7.37 us
    all_gather x1, blocking collectives, shards(): lax.all_gather(tokens, 'tp', axis=1, tiled=True)  6.85 us
    dot_general x1, matrix products, head_combiner(): jnp.einsum('shij,shj->shi', new_state, receptance_rows, precision=highest)  6.58 us
  transfers between devices with their start and end apart: 3, of which 3 were waited for; matrix products, arithmetic and copies ran while one was open for 1% of the time, Pallas kernels for 0%

commit v1 on v0

--- a/solution.py
+++ b/solution.py
@@ -142,8 +142,8 @@
     head_terms = jnp.dot(mixed_inputs, output_weight, preferred_element_type=jnp.float32)
     own_columns = tokens.shape[1]
     column_start = lax.axis_index("tp") * own_columns
-    residual = present_rows.astype(jnp.float32) + lax.psum(
-        head_terms.astype(jnp.bfloat16), "tp"
+    residual = present_rows.astype(jnp.float32) + jnp.sum(
+        lax.all_gather(head_terms.astype(jnp.bfloat16), "tp"), axis=0
     ).astype(jnp.float32)
     expert_rows = row_rescale(residual, second_norm_gain).astype(jnp.bfloat16)
     residual_own = lax.dynamic_slice_in_dim(residual, column_start, own_columns, 1)

time: 154 us -> 131 us (0.85)
  waiting for transfers between devices: 60.5 us -> 28.7 us
  blocking collectives: 33.3 us -> 42.8 us
    psum x1 -> x0, waiting for transfers between devices: 31.7 us -> none  [shards(): lax.psum(head_terms.astype(jnp.bfloat16), 'tp').astype(jnp.float32)]
    all_gather x0 -> x1, blocking collectives: none -> 7.37 us  [shards(): lax.all_gather(head_terms.astype(jnp.bfloat16), 'tp')]
  transfers between devices with their start and end apart: 3 -> 2, of which waited for: 3 -> 2; matrix products, arithmetic and copies ran while one was open for 1% -> 0% of each run, Pallas kernels for 0% -> 0%
where the time goes in v1:
time: 131 us
  blocking collectives  42.8 us (33%)
  waiting for transfers between devices  28.7 us (22%)
  matrix products  25.1 us (19%)
  between operations  14.4 us (11%)
  other arithmetic  7.07 us (5%)
  local copies, waits for them, and re-layouts  7.03 us (5%)
  starting transfers between devices  5.55 us (4%)
    reduce_scatter x1, waiting for transfers between devices, shards(): lax.psum_scatter(down_terms.astype(jnp.bfloat16), 'tp', scatter_dimension...  21.3 us
    all_to_all x1, blocking collectives, shards(): lax.all_to_all(outgoing, 'ep', split_axis=0, concat_axis=0, tiled=True)  14.2 us
    all_gather x1, blocking collectives, shards(): lax.all_gather(lax.all_to_all(outgoing, 'ep', split_axis=0, concat_axis=0...  8.58 us
    dot_general x1, matrix products, head_combiner(): along = jnp.einsum('shij,shj->shi', state, removal, precision=highest)  8.53 us
    all_to_all x1, waiting for transfers between devices, shards(): lax.all_to_all(shares, 'ep', split_axis=0, concat_axis=0, tiled=True)  7.37 us
    all_gather x1, blocking collectives, shards(): lax.all_gather(head_terms.astype(jnp.bfloat16), 'tp')  7.37 us
    all_gather x1, blocking collectives, shards(): lax.all_gather(tokens, 'tp', axis=1, tiled=True)  6.85 us
    dot_general x1, matrix products, head_combiner(): jnp.einsum('shij,shj->shi', new_state, receptance_rows, precision=highest)  6.58 us
  transfers between devices with their start and end apart: 2, of which 2 were waited for; matrix products, arithmetic and copies ran while one was open for 0% of the time, Pallas kernels for 0%

profile of v1, /device:TPU:0, one launch (start us, length us, event | category | flops | bytes accessed | tf_op | source)
XLA Modules:
  0.0 130.6 jit_solution(6139759820896175238)
XLA Ops:
  7.3 6.9 %all_gather.15 = bf16[32,2048]{1,0:T(8,128)(2,1)S(1)} all-gather(bf16[32,512]{1,0:T(8,128)(2,1)} %param.24), channel_id=1, replica_groups=mesh['ep'=8,'tp'=4] {'tp'}, dimensions={1}, use_global_device_ids=true | all-gather | bytes 163840 | tf_op jit(solution)/shard_map/all_gather | solution.py:116
  14.1 0.1 fusion.16
  14.3 5.8 %all_gather.16 = bf16[32,2048]{1,0:T(8,128)(2,1)S(1)} all-gather(bf16[32,512]{1,0:T(8,128)(2,1)} %param.25), channel_id=1, replica_groups=mesh['ep'=8,'tp'=4] {'tp'}, dimensions={1}, use_global_device_ids=true | all-gather | bytes 163840 | tf_op jit(solution)/shard_map/all_gather | solution.py:117
  20.1 1.1 fusion.83
  21.2 1.6 %fusion.29 = f32[32,256]{1,0:T(8,128)S(1)} fusion(bf16[2048,256]{1,0:T(8,128)(2,1)} %param.28, bf16[32,2048]{1,0:T(8,128)(2,1)S(1)} %all_gather.15, bf16[32,2048]{1,0:T(8,128)(2,1)S(1)} %all_gather.16, f32[2048]{0:T(1024)S(1)} %bitcast.62, f32[2048]{0:T(1024)} %param.26, f32[32]{0:T(128)S(1)} %add_rsqrt_fusion.3), kind=kOutput, calls=%fused_computation.45 | convolution fusion | flops 34078720 | bytes 1360000 | tf_op jit(solution)/shard_map/dot_general | solution.py:46
  22.7 0.1 reshape.177
  22.8 0.7 reshape.161
  23.5 1.4 %fusion.10 = f32[32,256]{1,0:T(8,128)S(1)} fusion(bf16[2048,128]{1,0:T(8,128)(2,1)} %param.34, bf16[32,2048]{1,0:T(8,128)(2,1)S(1)} %all_gather.15, bf16[32,2048]{1,0:T(8,128)(2,1)S(1)} %all_gather.16, f32[2048]{0:T(1024)S(1)} %bitcast.64, f32[2048]{0:T(1024)} %param.26, f32[32]{0:T(128)S(1)} %add_rsqrt_fusion.3, bf16[128,1024]{1,0:T(8,128)(2,1)} %param.35, ...), kind=kOutput, calls=%fused_computation.18 | convolution fusion | flops 19427328 | bytes 901252 | tf_op jit(solution)/shard_map/dot_general | solution.py:46
  25.0 0.1 reshape.160
  25.1 1.6 %fusion.35 = f32[32,256]{1,0:T(8,128)S(1)} fusion(bf16[2048,256]{1,0:T(8,128)(2,1)} %param.29, bf16[32,2048]{1,0:T(8,128)(2,1)S(1)} %all_gather.15, bf16[32,2048]{1,0:T(8,128)(2,1)S(1)} %all_gather.16, f32[2048]{0:T(1024)S(1)} %bitcast.61, f32[2048]{0:T(1024)} %param.26, f32[32]{0:T(128)S(1)} %add_rsqrt_fusion.3), kind=kOutput, calls=%fused_computation.47 | convolution fusion | flops 34078720 | bytes 1360000 | tf_op jit(solution)/shard_map/dot_general | solution.py:46
  26.6 0.1 reshape.159
  26.8 0.1 multiply_reduce_fusion.3
  27.1 1.3 fusion.67
  28.4 0.1 mul.284
  28.5 0.3 fusion.31
  28.8 0.1 mul.306
  28.9 0.1 fusion.82
  29.0 8.5 %fusion.84 = f32[32,4,1,64]{3,2,1,0:T(1,128)S(1)} fusion(f32[32,4,64,1]{2,3,1,0:T(1,128)S(1)} %bitcast.58, f32[32,4,64,64]{3,2,1,0:T(8,128)} %param.41), kind=kOutput, calls=%fused_computation.105 | convolution fusion | flops 6291456 | bytes 2162688 | tf_op jit(solution)/shard_map/shij,shj->shi/dot_general | solution.py:63
  37.5 2.7 %multiply_add_fusion = f32[32,4,64,64]{3,2,1,0:T(8,128)S(1)} fusion(f32[32,4,64,64]{3,2,1,0:T(8,128)S(1)} %copy-done.1, f32[32,4,64]{2,1,0:T(4,128)S(1)} %get-tuple-element.8, f32[32,4,64]{2,1,0:T(4,128)S(1)} %mul.306, f32[32,4,64]{2,1,0:T(4,128)S(1)} %get-tuple-element.4, f32[32,4,64]{2,1,0:T(4,128)S(1)} %bitcast.56, f32[32,4,64]{2,1,0:T(4,128)S(1)} %mul.284), kind=kLoop, calls=%fused_computation.2 | loop fusion | flops 2621440 | bytes 4358144 | tf_op jit(solution)/shard_map/add | solution.py:65
  40.4 2.0 %copy-done.2 = f32[32,4,64,64]{3,2,1,0:T(8,128)} copy-done((f32[32,4,64,64]{3,2,1,0:T(8,128)}, f32[32,4,64,64]{3,2,1,0:T(8,128)S(1)}, u32[]{:S(2)}) %copy-start.2) | copy-done | bytes 2097176
  42.3 6.6 %fusion.85 = f32[32,4,1,64]{3,2,1,0:T(1,128)S(1)} fusion(f32[32,4,64,64]{3,2,1,0:T(8,128)S(1)} %multiply_add_fusion, f32[32,4,64,1]{2,3,1,0:T(1,128)S(1)} %bitcast.57), kind=kOutput, calls=%fused_computation.106 | convolution fusion | flops 6291456 | bytes 2162688 | tf_op jit(solution)/shard_map/shij,shj->shi/dot_general | solution.py:69
  48.9 0.1 reduce_sum.99
  49.0 0.2 multiply_reduce_fusion.2
  49.2 0.6 add_rsqrt_fusion
  49.9 1.4 %fusion.7 = bf16[32,4,64]{2,1,0:T(4,128)(2,1)S(1)} fusion(f32[32,4,64]{2,1,0:T(4,128)S(1)} %mul.306, f32[32,4,64]{2,1,0:T(4,128)S(1)} %bitcast.55, f32[4,64]{1,0:T(4,128)S(1)} %mul.320, f32[32,4]{1,0:T(8,128)} %add_rsqrt_fusion, f32[32,4]{1,0:T(8,128)S(1)} %broadcast_multiply_fusion, f32[32,4,64]{2,1,0:T(4,128)} %reshape.161, ...), kind=kOutput, calls=%fused_computation.14 | output fusion | flops 65727 | bytes 150528 | tf_op jit(solution)/shard_map/mul | solution.py:78
  51.3 0.1 convert_element_type.80
  51.4 0.3 convolution_convert_fusion.1
  51.7 7.4 %all-gather = bf16[128,2048]{1,0:T(8,128)(2,1)S(1)} all-gather(bf16[32,2048]{1,0:T(8,128)(2,1)S(1)} %convolution_convert_fusion.1), channel_id=2, replica_groups=mesh['ep'=8,'tp'=4] {'tp'}, dimensions={0}, use_global_device_ids=true | all-gather | bytes 655360 | tf_op jit(solution)/shard_map/all_gather | solution.py:146
  59.1 0.2 multiply_reduce_fusion.1
  59.4 0.1 reshape.162
  59.6 0.2 reduce_window_sum.11
  59.8 0.2 select_reduce_fusion
  60.0 0.1 reduce_sum.104
  60.3 0.8 dynamic-slice
  61.0 0.2 convolution_convert_fusion.2
  61.3 14.2 %all_to_all.10 = bf16[8,24,512]{2,1,0:T(8,128)(2,1)S(1)} all-to-all(bf16[8,24,512]{2,1,0:T(8,128)(2,1)S(1)} %bitcast.52), channel_id=1, replica_groups=mesh['ep'=8,'tp'=4] {'ep'}, dimensions={0} | all-to-all | bytes 393216 | tf_op jit(solution)/shard_map/all_to_all | solution.py:167
  75.5 8.6 %all_gather.19 = bf16[8,24,2048]{2,1,0:T(8,128)(2,1)S(1)} all-gather(bf16[8,24,512]{2,1,0:T(8,128)(2,1)S(1)} %all_to_all.10), channel_id=1, replica_groups=mesh['ep'=8,'tp'=4] {'tp'}, dimensions={2}, use_global_device_ids=true | all-gather | bytes 983040 | tf_op jit(solution)/shard_map/all_gather | solution.py:166
  84.1 0.4 convolution_minimum_fusion
  84.5 1.6 %fusion.4 = bf16[192,256]{1,0:T(8,128)(2,1)S(1)} fusion(f32[192,256]{1,0:T(8,128)S(1)} %convolution_minimum_fusion, bf16[192,2048]{1,0:T(8,128)(2,1)S(1)} %bitcast.50, bf16[1,2048,256]{2,1,0:T(8,128)(2,1)} %param.46), kind=kOutput, calls=%fused_computation.11 | convolution fusion | flops 201768960 | bytes 2129920 | tf_op jit(solution)/shard_map/dot_general | solution.py:178
  86.1 1.3 convolution_convert_fusion
  87.4 21.3 %reduce-scatter.2.cloned.1.call-done = bf16[8,24,512]{2,1,0:T(8,128)(2,1)} async-done(((bf16[8,24,2048]{2,1,0:T(8,128)(2,1)}), bf16[8,24,512]{2,1,0:T(8,128)(2,1)}) %reduce-scatter.2.cloned.1.call-update) | async-done | bytes 196624 | tf_op jit(solution)/shard_map/reduce_scatter | solution.py:187
  108.7 5.5 %all-to-all-start.1 = ((bf16[8,24,512]{2,1,0:T(8,128)(2,1)}), bf16[8,24,512]{2,1,0:T(8,128)(2,1)S(1)}, u32[]{:S(2)}, u32[]{:S(2)}) async-start(bf16[8,24,512]{2,1,0:T(8,128)(2,1)} %reduce-scatter.2.cloned.1.call-done), calls=%async_computation.2 | async-start | bytes 393216 | tf_op jit(solution)/shard_map/all_to_all | solution.py:190
  114.3 0.1 mul.341
  114.4 0.1 copy.38
  114.6 7.4 %all-to-all-done.1 = bf16[8,24,512]{2,1,0:T(8,128)(2,1)S(1)} async-done(((bf16[8,24,512]{2,1,0:T(8,128)(2,1)}), bf16[8,24,512]{2,1,0:T(8,128)(2,1)S(1)}, u32[]{:S(2)}, u32[]{:S(2)}) %all-to-all-start.1) | async-done | bytes 196640 | tf_op jit(solution)/shard_map/all_to_all | solution.py:190
  122.0 0.8 gather_fusion
  122.9 0.3 multiply_reduce_fusion
  123.2 0.6 add_convert_fusion
  (50 shorter events, 1.1 us)
Async XLA Ops:
  7.2 78.9 %copy-start = (bf16[1,256,2048]{2,1,0:T(8,128)(2,1)S(1)}, bf16[1,256,2048]{2,1,0:T(8,128)(2,1)}, u32[]{:S(2)}) copy-start(bf16[1,256,2048]{2,1,0:T(8,128)(2,1)} %param.47) | copy-start | bytes 3145732
  7.2 19.9 %copy-start.6 = (f32[2048]{0:T(1024)S(1)}, f32[2048]{0:T(1024)}, u32[]{:S(2)}) copy-start(f32[2048]{0:T(1024)} %param.26) | copy-start | bytes 24580
  7.2 19.6 %copy-start.9 = (f32[256]{0:T(256)S(1)}, f32[256]{0:T(256)}, u32[]{:S(2)}) copy-start(f32[256]{0:T(256)} %param.36) | copy-start | bytes 3076
  7.2 19.8 %copy-start.10 = (f32[256]{0:T(256)S(1)}, f32[256]{0:T(256)}, u32[]{:S(2)}) copy-start(f32[256]{0:T(256)} %param.37) | copy-start | bytes 3076
  7.2 19.9 %copy-start.12 = (bf16[2048,128]{1,0:T(8,128)(2,1)S(1)}, bf16[2048,128]{1,0:T(8,128)(2,1)}, u32[]{:S(2)}) copy-start(bf16[2048,128]{1,0:T(8,128)(2,1)} %param.31) | copy-start | bytes 1572868
  7.2 19.8 %copy-start.14 = (f32[256]{0:T(256)S(1)}, f32[256]{0:T(256)}, u32[]{:S(2)}) copy-start(f32[256]{0:T(256)} %param.33) | copy-start | bytes 3076
  7.2 21.2 %copy-start.3 = (bf16[2048,256]{1,0:T(8,128)(2,1)S(1)}, bf16[2048,256]{1,0:T(8,128)(2,1)}, u32[]{:S(2)}) copy-start(bf16[2048,256]{1,0:T(8,128)(2,1)} %param.30) | copy-start | bytes 3145732
  7.2 101.5 %reduce-scatter.2.cloned.1.call-start = ((), (), s32[]{:S(2)}) async-start(), calls=%async_computation.3 | async-start | bytes 983040 | tf_op jit(solution)/shard_map/reduce_scatter | solution.py:187
  28.9 8.7 %copy-start.1 = (f32[32,4,64,64]{3,2,1,0:T(8,128)S(1)}, f32[32,4,64,64]{3,2,1,0:T(8,128)}, u32[]{:S(2)}) copy-start(f32[32,4,64,64]{3,2,1,0:T(8,128)} %param.41) | copy-start | bytes 6291460
  40.3 2.0 %copy-start.2 = (f32[32,4,64,64]{3,2,1,0:T(8,128)}, f32[32,4,64,64]{3,2,1,0:T(8,128)S(1)}, u32[]{:S(2)}) copy-start(f32[32,4,64,64]{3,2,1,0:T(8,128)S(1)} %multiply_add_fusion) | copy-start | bytes 6291460
  40.3 9.5 %copy-start.11 = (f32[256]{0:T(256)S(1)}, f32[256]{0:T(256)}, u32[]{:S(2)}) copy-start(f32[256]{0:T(256)} %param.39) | copy-start | bytes 3076
  40.3 9.6 %copy-start.13 = (f32[4,64]{1,0:T(4,128)S(1)}, f32[4,64]{1,0:T(4,128)}, u32[]{:S(2)}) copy-start(f32[4,64]{1,0:T(4,128)} %param.38) | copy-start | bytes 3076
  40.3 11.1 %copy-start.4 = (bf16[256,2048]{1,0:T(8,128)(2,1)S(1)}, bf16[256,2048]{1,0:T(8,128)(2,1)}, u32[]{:S(2)}) copy-start(bf16[256,2048]{1,0:T(8,128)(2,1)} %param.40) | copy-start | bytes 3145732
  40.3 19.0 %copy-start.7 = (s32[32,4]{0,1:T(4,128)S(1)}, s32[32,4]{0,1:T(4,128)}, u32[]{:S(2)}) copy-start(s32[32,4]{0,1:T(4,128)} %param.43) | copy-start | bytes 1540
  42.3 41.8 %copy-start.5 = (bf16[1,2048,256]{2,1,0:T(8,128)(2,1)S(1)}, bf16[1,2048,256]{2,1,0:T(8,128)(2,1)}, u32[]{:S(2)}) copy-start(bf16[1,2048,256]{2,1,0:T(8,128)(2,1)} %param.45) | copy-start | bytes 3145732
  84.1 30.5 %copy-start.8 = (f32[32,4]{0,1:T(4,128)S(1)}, f32[32,4]{0,1:T(4,128)}, u32[]{:S(2)}) copy-start(f32[32,4]{0,1:T(4,128)} %param.44) | copy-start | bytes 1540
  108.7 13.3 %all-to-all-start.1 = ((bf16[8,24,512]{2,1,0:T(8,128)(2,1)}), bf16[8,24,512]{2,1,0:T(8,128)(2,1)S(1)}, u32[]{:S(2)}, u32[]{:S(2)}) async-start(bf16[8,24,512]{2,1,0:T(8,128)(2,1)} %reduce-scatter.2.cloned.1.call-done), calls=%async_computation.2 | async-start | bytes 393216 | tf_op jit(solution)/shard_map/all_to_all | solution.py:190
Sparse Core Ops, SparseCore 0:
  87.5 21.1 reduce-scatter.1
